TPU v7x, 32 devices: a whole 2x2x4 slice. The times are simulated.
32 devices in a mesh: fs: 16 (over z, y, x), tp: 2 (over core).
Axes of the slice: x: 2, y: 2, z: 4, core: 2. Of those that a mesh axis runs over, the one named last changes fastest.
Arguments:
- saved_inputs: bfloat16 [12288, 2048], P('fs'), may hold values from -6 to 6
- cotangents: bfloat16 [3, 12288, 1024], P(None, 'fs', 'tp'), may hold values from -0.0546875 to 0.0546875
- left_roots: float32 [3, 2048, 2048], P(None, 'fs'), may hold values from -1 to 2
- right_roots: float32 [3, 1024, 128], P(None, 'tp'), may hold values from -1 to 2
- moments: float32 [3, 2048, 1024], P(None, 'fs', 'tp'), may hold values from -125 to 125
- masters: float32 [3, 2048, 1024], P(None, 'fs', 'tp'), may hold values from -3 to 3
Outputs:
- direction: float32 [3, 2048, 1024], P(None, 'fs', 'tp')
- moments_new: float32 [3, 2048, 1024], P(None, 'fs', 'tp')
- copies: bfloat16 [3, 2048, 1024], P(None, None, 'tp')
All inputs are finite; a program needn't handle non-finite values.
Results may differ from a plain program's by a relative error of at most 0.002.
Values may be sent and summed in bfloat16 or wider, within the bound.
A program may use at most 64 MiB of HBM per device.

v0:
```python
import jax
import jax.numpy as jnp
from jax import lax
from jax.sharding import PartitionSpec as P

D = 2048
SBW = 1024
RB = 128


momentum_decay = 0.9
step_rate = 0.1
eps_value = 1e-06


def on_device(saved_inputs, cotangents, left_roots, right_roots, moments, masters):
    rows_own = masters.shape[1]
    columns = masters.shape[2]
    grad_rows = lax.psum_scatter(
        jnp.einsum("td,mtc->dmc", saved_inputs, cotangents, preferred_element_type=jnp.float32),
        "fs",
        scatter_dimension=0,
        tiled=True,
    )
    empty = jnp.zeros((3, rows_own, columns), jnp.float32)
    left_done = empty + jnp.einsum(
        "mrn,nmc->mrc",
        left_roots,
        lax.all_gather(grad_rows.astype(jnp.bfloat16), "fs", axis=0, tiled=True).astype(
            jnp.float32
        ),
        precision=lax.Precision.HIGHEST,
    )
    block_count = columns // RB
    right_blocks = right_roots.reshape(3, block_count, RB, RB)
    right_done = jnp.einsum(
        "mrbi,mbij->mrbj",
        left_done.reshape(3, rows_own, block_count, RB),
        right_blocks,
        precision=lax.Precision.HIGHEST,
    ).reshape(3, rows_own, columns)
    moments_new = momentum_decay * moments + right_done
    totals = lax.psum(jnp.sum(moments_new * moments_new, axis=(1, 2)), ("fs", "tp"))
    meansq = totals / (D * SBW)
    direction = moments_new * lax.rsqrt(meansq + eps_value)[:, None, None]
    copy_rows = (masters - step_rate * direction).astype(jnp.bfloat16)
    copies = lax.all_gather(copy_rows, "fs", axis=1, tiled=True)
    return (direction, moments_new, copies)


def solution(mesh):
    placed = (
        P("fs", None),
        P(None, "fs", "tp"),
        P(None, "fs", None),
        P(None, "tp", None),
        P(None, "fs", "tp"),
        P(None, "fs", "tp"),
    )
    return jax.shard_map(
        on_device,
        mesh=mesh,
        in_specs=placed,
        out_specs=(P(None, "fs", "tp"), P(None, "fs", "tp"), P(None, None, "tp")),
        check_vma=False,
    )
```

profile of v0, /device:TPU:0, one launch (start us, length us, event | category | flops | bytes accessed | tf_op | source)
XLA Modules:
  0.0 505.3 jit_solution(11344276064925415366)
XLA Ops:
  7.2 0.0 copy-start
  7.2 0.0 reduce-scatter.2.cloned.1.call-start
  7.2 1.8 copy-done
  9.1 9.7 %fusion = f32[2048,3,512]{0,2,1:T(8,128)} fusion(bf16[3,768,512]{2,1,0:T(8,128)(2,1)} %param.7, bf16[768,2048]{1,0:T(8,128)(2,1)S(1)} %copy-done), kind=kOutput, calls=%fused_computation | convolution fusion | flops 4831838208 | bytes 18087936 | tf_op jit(solution)/shard_map/td,mtc->dmc/dot_general | solution.py:20
  18.7 0.0 reduce-scatter.2.cloned.1.call-update
  18.7 0.0 all-gather.3.cloned.1.call-start
  18.8 205.6 %reduce-scatter.2.cloned.1.call-done = f32[128,3,512]{0,2,1:T(8,128)} async-done(((f32[2048,3,512]{0,2,1:T(8,128)}), f32[128,3,512]{0,2,1:T(8,128)}) %reduce-scatter.2.cloned.1.call-update) | async-done | bytes 786448 | tf_op jit(solution)/shard_map/reduce_scatter | solution.py:19
  224.4 1.9 convert_element_type.7
  226.3 0.0 all-gather.3.cloned.1.call-update
  226.3 0.0 all-gather.5.cloned.1.call-start
  226.4 115.8 %all-gather.3.cloned.1.call-done = bf16[2048,3,512]{0,2,1:T(8,128)(2,1)} async-done(((bf16[128,3,512]{0,2,1:T(8,128)(2,1)}), bf16[2048,3,512]{0,2,1:T(8,128)(2,1)}) %all-gather.3.cloned.1.call-update) | async-done | bytes 6291472 | tf_op jit(solution)/shard_map/all_gather | solution.py:29
  342.2 0.0 copy-start.1
  342.2 8.4 %fusion.2 = f32[3,512,128]{2,1,0:T(8,128)S(1)} fusion(bf16[2048,3,512]{0,2,1:T(8,128)(2,1)} %all-gather.3.cloned.1.call-done, f32[3,128,2048]{2,1,0:T(8,128)} %param.8), kind=kOutput, calls=%fused_computation.7 | convolution fusion | flops 4831838208 | bytes 10223616 | tf_op jit(solution)/shard_map/mrn,nmc->mrc/dot_general | solution.py:26
  350.6 0.0 copy-done.1
  350.6 2.3 fusion.3
  352.9 2.3 copy.11
  355.2 2.4 multiply_reduce_fusion
  357.6 38.3 %psum.7 = f32[3]{0:T(128)S(1)} all-reduce(f32[3]{0:T(128)S(1)} %get-tuple-element.5), channel_id=1, replica_groups=mesh['fs'=16,'tp'=2] {'fs','tp'}, use_global_device_ids=true, to_apply=%region_2.0 | all-reduce | flops 3 | bytes 24 | tf_op jit(solution)/shard_map/psum | solution.py:43
  395.9 2.6 subtract_convert_fusion
  398.5 0.0 all-gather.5.cloned.1.call-update
  398.6 94.3 %all-gather.5.cloned.1.call-done = bf16[3,2048,512]{2,1,0:T(8,128)(2,1)} async-done(((bf16[3,128,512]{2,1,0:T(8,128)(2,1)}), bf16[3,2048,512]{2,1,0:T(8,128)(2,1)}) %all-gather.5.cloned.1.call-update) | async-done | bytes 6291472 | tf_op jit(solution)/shard_map/all_gather | solution.py:47
  492.9 5.9 %copy.15 = bf16[3,2048,512]{2,1,0:T(8,128)(2,1)} copy(bf16[3,2048,512]{2,1,0:T(8,128)(2,1)} %all-gather.5.cloned.1.call-done) | data formatting | bytes 12582912
  (1 shorter events, 0.0 us)
Async XLA Ops:
  7.2 1.9 copy-start
  7.2 217.2 %reduce-scatter.2.cloned.1.call-start = ((), (), s32[]{:S(2)}) async-start(), calls=%async_computation.1 | async-start | bytes 13369344 | tf_op jit(solution)/shard_map/reduce_scatter | solution.py:19
  18.7 323.4 %all-gather.3.cloned.1.call-start = ((), (), s32[]{:S(2)}) async-start(), calls=%async_computation.2 | async-start | bytes 6684672 | tf_op jit(solution)/shard_map/all_gather | solution.py:29
  226.3 266.5 %all-gather.5.cloned.1.call-start = ((), (), s32[]{:S(2)}) async-start(), calls=%async_computation.3 | async-start | bytes 6684672 | tf_op jit(solution)/shard_map/all_gather | solution.py:47
  342.2 8.4 %copy-start.1 = (f32[3,512,128]{2,1,0:T(8,128)S(1)}, f32[3,512,128]{2,1,0:T(8,128)}, u32[]{:S(2)}) copy-start(f32[3,512,128]{2,1,0:T(8,128)} %param.9) | copy-start | bytes 2359300
Sparse Core Ops, SparseCore 0:
  18.9 205.4 reduce-scatter.1
  227.7 114.4 all-gather.2
  398.7 94.1 all-gather.4
where the time goes:
time: 506 us; the launch traced here: 505 us
  waiting for transfers between devices  416 us (82%)
  blocking collectives  38.3 us (8%)
  matrix products  20.4 us (4%)
  between operations  13.8 us (3%)
  local copies, waits for them, and re-layouts  10 us (2%)
  other arithmetic  6.93 us (1%)
    reduce_scatter x1, waiting for transfers between devices, on_device(): lax.psum_scatter(jnp.einsum('td,mtc->dmc', saved_inputs, cotangents, pref...  206 us
    all_gather x1, waiting for transfers between devices, on_device(): lax.all_gather(grad_rows.astype(jnp.bfloat16), 'fs', axis=0, tiled=True)  116 us
    all_gather x1, waiting for transfers between devices, on_device(): copies = lax.all_gather(copy_rows, 'fs', axis=1, tiled=True)  94.3 us
    psum x1, blocking collectives, on_device(): lax.psum(jnp.sum(moments_new * moments_new, axis=(1, 2)), ('fs', 'tp'))  38.3 us
  transfers between devices with their start and end apart: 3, of which 3 were waited for; matrix products, arithmetic and copies ran while one was open for 0% of the time, Pallas kernels for 0%

commit v1 on v0

v1 whole, which is shorter than its diff:
```python
import functools

import jax
import jax.numpy as jnp
from jax import lax
from jax.experimental import pallas as pl
from jax.experimental.pallas import tpu as pltpu
from jax.sharding import PartitionSpec as P

RB = 128
momentum_decay = 0.9
step_rate = 0.1
eps_value = 1e-06
MESH = pl.DeviceIdType.MESH
F32 = jnp.float32
BF16 = jnp.bfloat16


def step_kernel(
    n, tpn, x_ref, c_ref, l_ref, r_ref, mom_ref, mas_ref, dir_ref, mnew_ref, out_ref,
    gp, r1, t1, r2, t2, r3, acc, gf, cf, own, st1, st2, mid,
    s_first, s_second, s_third, a_first, a_second, a_third, q_row, q_col, out_sem,
):
    g = n // 4
    count, rows, cols = mom_ref.shape
    depth = x_ref.shape[1]
    half = rows // 2
    me = lax.axis_index("fs")
    tp = lax.axis_index("tp")
    z, y, x = me // 4, (me // 2) % 2, me % 2
    y_peer, x_peer = me + 2 - 4 * y, me + 1 - 2 * x
    near = ((y, x, y_peer, x_peer), (x, y, x_peer, y_peer))

    def block(ref, m, h, zi, p, q):
        return ref.at[m, zi, p, q, h] if h == 0 else ref.at[m, zi, q, p, h]

    def pair(ref, m, h, zi, p):
        return ref.at[m, zi, p, :, h] if h == 0 else ref.at[m, zi, :, p, h]

    def remote(src, dst, sems, at, peer, axis="fs"):
        return pltpu.make_async_remote_copy(
            src_ref=src, dst_ref=dst, send_sem=sems.at[(0,) + at], recv_sem=sems.at[(1,) + at],
            device_id={axis: peer}, device_id_type=MESH,
        )

    def loop(low, high, body):
        def step(i, carry):
            body(i)
            return carry

        lax.fori_loop(low, high, step, 0)

    def around(d):
        return (z + d) % g

    def first(m, h, zi):
        p, _, peer, _ = near[h]
        return remote(pair(gp, m, h, zi, 1 - p), r1.at[m, h, zi], s_first, (m, h, zi), peer)

    def second(m, h, zi):
        return remote(t1.at[m, h, zi], r2.at[m, h, zi], s_second, (m, h, zi), near[h][3])

    def third(m, h, d):
        return remote(t2.at[m, h, d], r3.at[m, h, d], s_third, (m, h, d), around(d) * 4 + y * 2 + x)

    def value(m, h, zi, q):
        p = near[h][0]
        return block(gp, m, h, zi, p, q)[...].astype(F32) + r1[m, h, zi, q].astype(F32)

    def stage_partial(m):
        wide = 4 * rows

        def body(zi):
            part = lax.dot_general(
                x_ref[:, pl.ds(pl.multiple_of(zi * wide, wide), wide)], c_ref[m],
                (((0,), (0,)), ((), ())), preferred_element_type=F32,
            )
            gp[m, zi] = part.astype(BF16).reshape(2, 2, 2, half, cols)
            first(m, 0, zi).start()
            first(m, 1, zi).start()

        loop(0, g, body)

    def stage_second(m):
        def body(zi):
            for h in range(2):
                q = near[h][1]
                first(m, h, zi).wait_recv()
                t1[m, h, zi] = value(m, h, zi, 1 - q).astype(BF16)
                second(m, h, zi).start()

        loop(0, g, body)

    def stage_third(m):
        def reduced(h, zi):
            second(m, h, zi).wait_recv()
            return value(m, h, zi, near[h][1]) + r2[m, h, zi].astype(F32)

        def body(d):
            for h in range(2):
                t2[m, h, d] = reduced(h, around(d)).astype(BF16)
                third(m, h, d).start()

        loop(1, g, body)
        for h in range(2):
            acc[h] = reduced(h, z)

    def spread(k, buf, m, h, d):
        slot = block(buf, m, h, z, *near[h][:2])
        return remote(slot, slot, a_first, (k, m, h, d), around(d) * 4 + y * 2 + x)

    def across(k, buf, m, h, d):
        slot = block(buf, m, h, around(g - d), *near[h][:2])
        return remote(slot, slot, a_second, (k, m, h, d), near[h][3])

    def last(k, buf, m, h, d):
        slot = pair(buf, m, h, around(g - d), near[h][0])
        return remote(slot, slot, a_third, (k, m, h, d), near[h][2])

    def landed_spread(k, buf, m, h, d):
        slot = block(buf, m, h, around(g - d), *near[h][:2])
        return remote(slot, slot, a_first, (k, m, h, d), around(g - d) * 4 + y * 2 + x)

    def landed_across(k, buf, m, h, d):
        p, q, _, peer = near[h]
        slot = block(buf, m, h, around(g - d), p, 1 - q)
        return remote(slot, slot, a_second, (k, m, h, d), peer)

    def landed_last(k, buf, m, h, d):
        p, _, peer, _ = near[h]
        slot = pair(buf, m, h, around(g - d), 1 - p)
        return remote(slot, slot, a_third, (k, m, h, d), peer)

    def gather_start(k, buf, m):
        for h in range(2):
            across(k, buf, m, h, 0).start()

        def body(d):
            for h in range(2):
                spread(k, buf, m, h, d).start()

        loop(1, g, body)

    def gather_across(k, buf, m):
        def body(d):
            for h in range(2):
                landed_spread(k, buf, m, h, d).wait_recv()
                across(k, buf, m, h, d).start()

        loop(1, g, body)

    def gather_last(k, buf, m):
        def body(d):
            for h in range(2):
                landed_across(k, buf, m, h, d).wait_recv()
                last(k, buf, m, h, d).start()

        loop(0, g, body)

    def gather_wait(k, buf, m):
        def body(d):
            for h in range(2):
                landed_last(k, buf, m, h, d).wait_recv()

        loop(0, g, body)

    def stage_rows(m):
        def body(d):
            for h in range(2):
                third(m, h, d).wait_recv()
                acc[h] += r3[m, h, d].astype(F32)

        loop(1, g, body)
        for h in range(2):
            gf[m, z, y, x, h] = acc[h].astype(BF16)
        gather_start(0, gf, m)

    def row_sum(m, d):
        return remote(own.at[m], st1.at[m, d], q_row, (m, d), (me + d) % n)

    def col_sum(m, d):
        return remote(mid.at[m], st2.at[m, d], q_col, (m, d), (tp + d) % tpn, "tp")

    def stage_product(m):
        gather_wait(0, gf, m)
        roots = l_ref[m]
        high = roots.astype(BF16)
        low = (roots - high.astype(F32)).astype(BF16)
        both = jnp.dot(
            jnp.concatenate([high, low], axis=0), gf[m].reshape(depth, cols),
            preferred_element_type=F32,
        )
        left = both[:rows] + both[rows:]
        tile = jnp.zeros((8, RB), F32)
        for b in range(cols // RB):
            at = slice(b * RB, (b + 1) * RB)
            right = jnp.dot(
                left[:, at], r_ref[m, at, :], precision=lax.Precision.HIGHEST,
                preferred_element_type=F32,
            )
            new = momentum_decay * mom_ref[m, :, at] + right
            mnew_ref[m, :, at] = new
            tile += jnp.sum((new * new).reshape(rows // 8, 8, RB), axis=0)
        own[m] = tile
        loop(1, n, lambda d: row_sum(m, d).start())

    def stage_sum(m):
        loop(1, n, lambda d: row_sum(m, d).wait_recv())
        mid[m] = own[m] + jnp.sum(st1[m, 1:], axis=0)
        loop(1, tpn, lambda d: col_sum(m, d).start())

    def stage_copies(m):
        loop(1, tpn, lambda d: col_sum(m, d).wait_recv())
        tile = mid[m] + jnp.sum(st2[m, 1:], axis=0)
        total = jnp.sum(jnp.sum(tile, axis=1, keepdims=True), axis=0, keepdims=True)
        scale = lax.rsqrt(total / (depth * cols * tpn) + eps_value)
        direction = mnew_ref[m] * scale
        dir_ref[m] = direction
        cf[m, z, y, x] = (mas_ref[m] - step_rate * direction).astype(BF16).reshape(2, half, cols)
        gather_start(1, cf, m)

    def put(m):
        return pltpu.make_async_copy(cf.at[m], out_ref.at[m], out_sem.at[m])

    def stage_put(m):
        gather_wait(1, cf, m)
        put(m).start()

    stages = (
        stage_partial, stage_second, stage_third, stage_rows,
        functools.partial(gather_across, 0, gf), functools.partial(gather_last, 0, gf),
        stage_product, stage_sum, stage_copies,
        functools.partial(gather_across, 1, cf), functools.partial(gather_last, 1, cf), stage_put,
    )
    for t in range(len(stages) + count - 1):
        if t < count:
            stages[0](t)
        for m in range(min(t, count)):
            if t - m < len(stages):
                stages[t - m](m)

    for m in range(count):
        put(m).wait()

        def sent(d):
            for h in range(2):
                first(m, h, d).wait_send()
                second(m, h, d).wait_send()
                for k, buf in ((0, gf), (1, cf)):
                    across(k, buf, m, h, d).wait_send()
                    last(k, buf, m, h, d).wait_send()

        def sent_far(d):
            for h in range(2):
                third(m, h, d).wait_send()
                for k, buf in ((0, gf), (1, cf)):
                    spread(k, buf, m, h, d).wait_send()

        loop(0, g, sent)
        loop(1, g, sent_far)
        loop(1, n, lambda d: row_sum(m, d).wait_send())
        loop(1, tpn, lambda d: col_sum(m, d).wait_send())


def on_device(n, tpn, saved_inputs, cotangents, left_roots, right_roots, moments, masters):
    g = n // 4
    count, rows, cols = moments.shape
    depth = saved_inputs.shape[1]
    half = rows // 2
    vmem = pl.BlockSpec(memory_space=pltpu.VMEM)
    grid_shape = (count, g, 2, 2, 2, half, cols)
    dma = pltpu.SemaphoreType.DMA
    direction, moments_new, copies = pl.pallas_call(
        functools.partial(step_kernel, n, tpn),
        out_shape=(
            jax.ShapeDtypeStruct(moments.shape, F32),
            jax.ShapeDtypeStruct(moments.shape, F32),
            jax.ShapeDtypeStruct(grid_shape, BF16),
        ),
        in_specs=[vmem] * 6,
        out_specs=(vmem, vmem, pl.BlockSpec(memory_space=pl.ANY)),
        scratch_shapes=[
            pltpu.VMEM(grid_shape, BF16),
            pltpu.VMEM((count, 2, g, 2, half, cols), BF16),
            pltpu.VMEM((count, 2, g, half, cols), BF16),
            pltpu.VMEM((count, 2, g, half, cols), BF16),
            pltpu.VMEM((count, 2, g, half, cols), BF16),
            pltpu.VMEM((count, 2, g, half, cols), BF16),
            pltpu.VMEM((2, half, cols), F32),
            pltpu.VMEM(grid_shape, BF16),
            pltpu.VMEM(grid_shape, BF16),
            pltpu.VMEM((count, 8, RB), F32),
            pltpu.VMEM((count, n, 8, RB), F32),
            pltpu.VMEM((count, tpn, 8, RB), F32),
            pltpu.VMEM((count, 8, RB), F32),
            dma((2, count, 2, g)), dma((2, count, 2, g)), dma((2, count, 2, g)),
            dma((2, 2, count, 2, g)), dma((2, 2, count, 2, g)), dma((2, 2, count, 2, g)),
            dma((2, count, n)), dma((2, count, tpn)), dma((count,)),
        ],
        compiler_params=pltpu.CompilerParams(
            has_side_effects=True, vmem_limit_bytes=64000 * 1024
        ),
        name="step",
    )(saved_inputs, cotangents, left_roots, right_roots, moments, masters)
    return direction, moments_new, copies.reshape(count, depth, cols)


def solution(mesh):
    placed = (
        P("fs", None),
        P(None, "fs", "tp"),
        P(None, "fs", None),
        P(None, "tp", None),
        P(None, "fs", "tp"),
        P(None, "fs", "tp"),
    )
    return jax.shard_map(
        functools.partial(on_device, mesh.shape["fs"], mesh.shape["tp"]),
        mesh=mesh,
        in_specs=placed,
        out_specs=(P(None, "fs", "tp"), P(None, "fs", "tp"), P(None, None, "tp")),
        check_vma=False,
    )
```

time: 506 us -> 206 us (0.41)
  waiting for transfers between devices: 416 us -> 0 us
  Pallas kernels: 0 us -> 195 us
  blocking collectives: 38.3 us -> 0 us
  matrix products: 20.4 us -> 0 us
  between operations: 13.8 us -> 0.64 us
  other arithmetic: 6.93 us -> 0 us
    all_gather x2 -> x0, waiting for transfers between devices: 210 us -> none  [the longest x1 116 us: on_device(): lax.all_gather(grad_rows.astype(jnp.bfloat16), 'fs', axis=0, tiled=True)]
    reduce_scatter x1 -> x0, waiting for transfers between devices: 206 us -> none  [on_device(): lax.psum_scatter(jnp.einsum('td,mtc->dmc', saved_inputs, cotangents, pref...]
    pallas_call x0 -> x1, Pallas kernels: none -> 195 us  [on_device(): pl.pallas_call(functools.partial(step_kernel, n, tpn), out_shape=(jax.Sha...]
    psum x1 -> x0, blocking collectives: 38.3 us -> none  [on_device(): lax.psum(jnp.sum(moments_new * moments_new, axis=(1, 2)), ('fs', 'tp'))]
    dot_general x3 -> x0, matrix products: 20.4 us -> none  [the longest x1 9.66 us: on_device(): jnp.einsum('td,mtc->dmc', saved_inputs, cotangents, preferred_element_typ...]
  transfers between devices with their start and end apart: 3 -> 0, of which waited for: 3 -> 0; matrix products, arithmetic and copies ran while one was open for 0% -> 0% of each run, Pallas kernels for 0% -> 0%
where the time goes in v1:
time: 206 us
  Pallas kernels  195 us (95%)
  local copies, waits for them, and re-layouts  10 us (5%)
    pallas_call x1, Pallas kernels, on_device(): pl.pallas_call(functools.partial(step_kernel, n, tpn), out_shape=(jax.Sha...  195 us
    unnamed x3, local copies, waits for them, and re-layouts  10 us

profile of v1, /device:TPU:0, one launch (start us, length us, event | category | flops | bytes accessed | tf_op | source)
XLA Modules:
  0.0 206.0 jit_solution(1953773987860024380)
XLA Ops:
  0.6 195.3 %step.1 = (f32[3,128,512]{2,1,0:T(8,128)}, f32[3,128,512]{2,1,0:T(8,128)}, bf16[3,4,2,2,2,64,512]{6,5,4,3,2,1,0:T(8,128)(2,1)}) custom-call(bf16[768,2048]{1,0:T(8,128)(2,1)} %x_ref.1, bf16[3,768,512]{2,1,0:T(8,128)(2,1)} %c_ref.1, f32[3,128,2048]{2,1,0:T(8,128)} %l_ref.1, f32[3,512,128]{2,1,0:T(8,128)} %r_ref.1, f32[3,128,512]{2,1,0:T(8,128)} %mom_ref.1, ...), custom_call_target="tpu_custom_call" | custom-call | tf_op jit(solution)/shard_map/step/pallas_call | solution.py:273
  195.9 2.1 %copy.12 = f32[3,128,512]{2,1,0:T(8,128)} copy(f32[3,128,512]{2,1,0:T(8,128)} %get-tuple-element.12) | data formatting | bytes 1572864
  198.0 2.1 %copy.13 = f32[3,128,512]{2,1,0:T(8,128)} copy(f32[3,128,512]{2,1,0:T(8,128)} %get-tuple-element.13) | data formatting | bytes 1572864
  200.1 5.9 %copy.14 = bf16[3,2048,512]{2,1,0:T(8,128)(2,1)} copy(bf16[3,2048,512]{2,1,0:T(8,128)(2,1)} %bitcast.1) | data formatting | bytes 12582912

commit v2 on v1

--- a/solution.py
+++ b/solution.py
@@ -17,14 +17,18 @@
 
 
 def step_kernel(
-    n, tpn, x_ref, c_ref, l_ref, r_ref, mom_ref, mas_ref, dir_ref, mnew_ref, out_ref,
-    gp, r1, t1, r2, t2, r3, acc, gf, cf, own, st1, st2, mid,
-    s_first, s_second, s_third, a_first, a_second, a_third, q_row, q_col, out_sem,
+    n, tpn, x_in, c_in, l_in, r_in, mom_in, mas_in, dir_ref, mnew_ref, cf,
+    x_ref, c_ref, l_ref, r_ref, mom_ref, mas_ref,
+    gp, r1, t1, r2, t2, r3, acc, t2b, r3b, accb, gf, own, st1, st2, mid,
+    s_first, s_second, s_third, a_first, a_second, a_third, a_fourth, q_row, q_col,
+    x_sem, c_sem, in_sem,
 ):
     g = n // 4
     count, rows, cols = mom_ref.shape
     depth = x_ref.shape[1]
     half = rows // 2
+    wide = 4 * rows
+    far_first = -1
     me = lax.axis_index("fs")
     tp = lax.axis_index("tp")
     z, y, x = me // 4, (me // 2) % 2, me % 2
@@ -67,10 +71,32 @@
         p = near[h][0]
         return block(gp, m, h, zi, p, q)[...].astype(F32) + r1[m, h, zi, q].astype(F32)
 
+    def load_x(zi):
+        at = pl.ds(pl.multiple_of(zi * wide, wide), wide)
+        return pltpu.make_async_copy(x_in.at[:, at], x_ref.at[:, at], x_sem.at[zi])
+
+    def load_c(m):
+        return pltpu.make_async_copy(c_in.at[m], c_ref.at[m], c_sem.at[m])
+
+    later = (
+        pltpu.make_async_copy(l_in, l_ref, in_sem.at[0]),
+        pltpu.make_async_copy(r_in, r_ref, in_sem.at[1]),
+        pltpu.make_async_copy(mom_in, mom_ref, in_sem.at[2]),
+        pltpu.make_async_copy(mas_in, mas_ref, in_sem.at[3]),
+    )
+    load_c(0).start()
+    loop(0, g, lambda zi: load_x(zi).start())
+    for m in range(1, count):
+        load_c(m).start()
+    for copy in later:
+        copy.start()
+
     def stage_partial(m):
-        wide = 4 * rows
+        load_c(m).wait()
 
         def body(zi):
+            if m == 0:
+                load_x(zi).wait()
             part = lax.dot_general(
                 x_ref[:, pl.ds(pl.multiple_of(zi * wide, wide), wide)], c_ref[m],
                 (((0,), (0,)), ((), ())), preferred_element_type=F32,
@@ -81,7 +107,40 @@
 
         loop(0, g, body)
 
+    def third_wide(h, d):
+        peer = around(d) * 4 + y * 2 + x
+        return remote(t2b.at[h, d], r3b.at[h, d], s_third, (far_first, h, d), peer)
+
+    def stage_second_far(m):
+        def summed(h, zi):
+            first(m, h, zi).wait_recv()
+            kept = pair(gp, m, h, zi, near[h][0])[...].astype(F32)
+            return kept + r1[m, h, zi].astype(F32)
+
+        def body(d):
+            for h in range(2):
+                t2b[h, d] = summed(h, around(d)).astype(BF16)
+                third_wide(h, d).start()
+
+        loop(1, g, body)
+        for h in range(2):
+            accb[h] = summed(h, z)
+
+    def stage_third_far(m):
+        def body(d):
+            for h in range(2):
+                third_wide(h, d).wait_recv()
+                accb[h] += r3b[h, d].astype(F32)
+
+        loop(1, g, body)
+        for h in range(2):
+            t1[m, h, 0] = accb[h, 1 - near[h][1]].astype(BF16)
+            second(m, h, 0).start()
+
     def stage_second(m):
+        if m == far_first:
+            return stage_second_far(m)
+
         def body(zi):
             for h in range(2):
                 q = near[h][1]
@@ -92,6 +151,9 @@
         loop(0, g, body)
 
     def stage_third(m):
+        if m == far_first:
+            return stage_third_far(m)
+
         def reduced(h, zi):
             second(m, h, zi).wait_recv()
             return value(m, h, zi, near[h][1]) + r2[m, h, zi].astype(F32)
@@ -141,7 +203,42 @@
 
         loop(1, g, body)
 
+    def spread_near(k, buf, m, h, d):
+        p, q, _, _ = near[h]
+        slot = block(buf, m, h, z, p, 1 - q)
+        return remote(slot, slot, a_fourth, (k, h, d), around(d) * 4 + y * 2 + x)
+
+    def landed_spread_near(k, buf, m, h, d):
+        p, q, _, _ = near[h]
+        slot = block(buf, m, h, around(g - d), p, 1 - q)
+        return remote(slot, slot, a_fourth, (k, h, d), around(g - d) * 4 + y * 2 + x)
+
+    def gather_across_far(k, buf, m):
+        for h in range(2):
+            landed_across(k, buf, m, h, 0).wait_recv()
+
+        def body(d):
+            for h in range(2):
+                spread_near(k, buf, m, h, d).start()
+
+        loop(1, g, body)
+
+    def gather_last_far(k, buf, m):
+        for h in range(2):
+            last(k, buf, m, h, 0).start()
+
+        def body(d):
+            for h in range(2):
+                landed_spread(k, buf, m, h, d).wait_recv()
+                landed_spread_near(k, buf, m, h, d).wait_recv()
+                last(k, buf, m, h, d).start()
+
+        loop(1, g, body)
+
     def gather_across(k, buf, m):
+        if m == far_first:
+            return gather_across_far(k, buf, m)
+
         def body(d):
             for h in range(2):
                 landed_spread(k, buf, m, h, d).wait_recv()
@@ -150,6 +247,9 @@
         loop(1, g, body)
 
     def gather_last(k, buf, m):
+        if m == far_first:
+            return gather_last_far(k, buf, m)
+
         def body(d):
             for h in range(2):
                 landed_across(k, buf, m, h, d).wait_recv()
@@ -170,9 +270,14 @@
                 third(m, h, d).wait_recv()
                 acc[h] += r3[m, h, d].astype(F32)
 
-        loop(1, g, body)
-        for h in range(2):
-            gf[m, z, y, x, h] = acc[h].astype(BF16)
+        if m != far_first:
+            loop(1, g, body)
+        for h in range(2):
+            if m == far_first:
+                second(m, h, 0).wait_recv()
+                gf[m, z, y, x, h] = (accb[h, near[h][1]] + r2[m, h, 0].astype(F32)).astype(BF16)
+            else:
+                gf[m, z, y, x, h] = acc[h].astype(BF16)
         gather_start(0, gf, m)
 
     def row_sum(m, d):
@@ -183,6 +288,9 @@
 
     def stage_product(m):
         gather_wait(0, gf, m)
+        if m == 0:
+            for copy in later:
+                copy.wait()
         roots = l_ref[m]
         high = roots.astype(BF16)
         low = (roots - high.astype(F32)).astype(BF16)
@@ -219,47 +327,57 @@
         cf[m, z, y, x] = (mas_ref[m] - step_rate * direction).astype(BF16).reshape(2, half, cols)
         gather_start(1, cf, m)
 
-    def put(m):
-        return pltpu.make_async_copy(cf.at[m], out_ref.at[m], out_sem.at[m])
-
-    def stage_put(m):
-        gather_wait(1, cf, m)
-        put(m).start()
-
     stages = (
         stage_partial, stage_second, stage_third, stage_rows,
         functools.partial(gather_across, 0, gf), functools.partial(gather_last, 0, gf),
         stage_product, stage_sum, stage_copies,
-        functools.partial(gather_across, 1, cf), functools.partial(gather_last, 1, cf), stage_put,
+        functools.partial(gather_across, 1, cf), functools.partial(gather_last, 1, cf),
+        functools.partial(gather_wait, 1, cf),
     )
-    for t in range(len(stages) + count - 1):
-        if t < count:
-            stages[0](t)
-        for m in range(min(t, count)):
-            if t - m < len(stages):
-                stages[t - m](m)
+    skew = 2
+    order = sorted((i + skew * m, i > 0, m, i) for m in range(count) for i in range(len(stages)))
+    for _, _, m, i in order:
+        stages[i](m)
 
     for m in range(count):
-        put(m).wait()
+        far = m == far_first
 
         def sent(d):
             for h in range(2):
                 first(m, h, d).wait_send()
+                for k, buf in ((0, gf), (1, cf)):
+                    last(k, buf, m, h, d).wait_send()
+
+        def sent_second(d):
+            for h in range(2):
                 second(m, h, d).wait_send()
                 for k, buf in ((0, gf), (1, cf)):
                     across(k, buf, m, h, d).wait_send()
-                    last(k, buf, m, h, d).wait_send()
 
         def sent_far(d):
             for h in range(2):
-                third(m, h, d).wait_send()
+                (third_wide(h, d) if far else third(m, h, d)).wait_send()
                 for k, buf in ((0, gf), (1, cf)):
                     spread(k, buf, m, h, d).wait_send()
+                    if far:
+                        spread_near(k, buf, m, h, d).wait_send()
 
         loop(0, g, sent)
+        loop(0, 1 if far else g, sent_second)
         loop(1, g, sent_far)
         loop(1, n, lambda d: row_sum(m, d).wait_send())
         loop(1, tpn, lambda d: col_sum(m, d).wait_send())
+
+
+def put_kernel(dir_ref, mnew_ref, cf, dir_out, mnew_out, cf_out, sem):
+    copies = [
+        pltpu.make_async_copy(src, dst, sem.at[i])
+        for i, (src, dst) in enumerate(((cf, cf_out), (dir_ref, dir_out), (mnew_ref, mnew_out)))
+    ]
+    for copy in copies:
+        copy.start()
+    for copy in copies:
+        copy.wait()
 
 
 def on_device(n, tpn, saved_inputs, cotangents, left_roots, right_roots, moments, masters):
@@ -268,18 +386,25 @@
     depth = saved_inputs.shape[1]
     half = rows // 2
     vmem = pl.BlockSpec(memory_space=pltpu.VMEM)
+    anywhere = pl.BlockSpec(memory_space=pl.ANY)
     grid_shape = (count, g, 2, 2, 2, half, cols)
     dma = pltpu.SemaphoreType.DMA
     direction, moments_new, copies = pl.pallas_call(
         functools.partial(step_kernel, n, tpn),
         out_shape=(
-            jax.ShapeDtypeStruct(moments.shape, F32),
-            jax.ShapeDtypeStruct(moments.shape, F32),
-            jax.ShapeDtypeStruct(grid_shape, BF16),
+            pltpu.VMEM(moments.shape, F32),
+            pltpu.VMEM(moments.shape, F32),
+            pltpu.VMEM(grid_shape, BF16),
         ),
-        in_specs=[vmem] * 6,
-        out_specs=(vmem, vmem, pl.BlockSpec(memory_space=pl.ANY)),
+        in_specs=[anywhere] * 6,
+        out_specs=(vmem, vmem, vmem),
         scratch_shapes=[
+            pltpu.VMEM(saved_inputs.shape, BF16),
+            pltpu.VMEM(cotangents.shape, BF16),
+            pltpu.VMEM(left_roots.shape, F32),
+            pltpu.VMEM(right_roots.shape, F32),
+            pltpu.VMEM(moments.shape, F32),
+            pltpu.VMEM(masters.shape, F32),
             pltpu.VMEM(grid_shape, BF16),
             pltpu.VMEM((count, 2, g, 2, half, cols), BF16),
             pltpu.VMEM((count, 2, g, half, cols), BF16),
@@ -287,7 +412,9 @@
             pltpu.VMEM((count, 2, g, half, cols), BF16),
             pltpu.VMEM((count, 2, g, half, cols), BF16),
             pltpu.VMEM((2, half, cols), F32),
-            pltpu.VMEM(grid_shape, BF16),
+            pltpu.VMEM((2, g, 2, half, cols), BF16),
+            pltpu.VMEM((2, g, 2, half, cols), BF16),
+            pltpu.VMEM((2, 2, half, cols), F32),
             pltpu.VMEM(grid_shape, BF16),
             pltpu.VMEM((count, 8, RB), F32),
             pltpu.VMEM((count, n, 8, RB), F32),
@@ -295,13 +422,28 @@
             pltpu.VMEM((count, 8, RB), F32),
             dma((2, count, 2, g)), dma((2, count, 2, g)), dma((2, count, 2, g)),
             dma((2, 2, count, 2, g)), dma((2, 2, count, 2, g)), dma((2, 2, count, 2, g)),
-            dma((2, count, n)), dma((2, count, tpn)), dma((count,)),
+            dma((2, 2, 2, g)),
+            dma((2, count, n)), dma((2, count, tpn)),
+            dma((g,)), dma((count,)), dma((4,)),
         ],
         compiler_params=pltpu.CompilerParams(
-            has_side_effects=True, vmem_limit_bytes=64000 * 1024
+            has_side_effects=True, vmem_limit_bytes=52000 * 1024
         ),
         name="step",
     )(saved_inputs, cotangents, left_roots, right_roots, moments, masters)
+    direction, moments_new, copies = pl.pallas_call(
+        put_kernel,
+        out_shape=(
+            jax.ShapeDtypeStruct(moments.shape, F32),
+            jax.ShapeDtypeStruct(moments.shape, F32),
+            jax.ShapeDtypeStruct(grid_shape, BF16),
+        ),
+        in_specs=[vmem] * 3,
+        out_specs=(anywhere,) * 3,
+        scratch_shapes=[dma((3,))],
+        compiler_params=pltpu.CompilerParams(vmem_limit_bytes=4096 * 1024),
+        name="put",
+    )(direction, moments_new, copies)
     return direction, moments_new, copies.reshape(count, depth, cols)
 
 

time: 206 us -> 186 us (0.903)
  Pallas kernels: 195 us -> 185 us
  local copies, waits for them, and re-layouts: 10 us -> 0 us
    pallas_call x1 -> x2, Pallas kernels: 195 us -> 185 us  [the longest x1 182 us: on_device(): pl.pallas_call(functools.partial(step_kernel, n, tpn), out_shape=(pltpu.V...]
    unnamed x3 -> x0, local copies, waits for them, and re-layouts: 10 us -> none
where the time goes in v2:
time: 186 us
  Pallas kernels  185 us (99%)
    pallas_call x1, Pallas kernels, on_device(): pl.pallas_call(functools.partial(step_kernel, n, tpn), out_shape=(pltpu.V...  182 us

profile of v2, /device:TPU:0, one launch (start us, length us, event | category | flops | bytes accessed | tf_op | source)
XLA Modules:
  0.0 185.5 jit_solution(18025856684032764681)
XLA Ops:
  0.6 181.7 %step.1 = (f32[3,128,512]{2,1,0:T(8,128)S(1)}, f32[3,128,512]{2,1,0:T(8,128)S(1)}, bf16[3,4,2,2,2,64,512]{6,5,4,3,2,1,0:T(8,128)(2,1)S(1)}) custom-call(bf16[768,2048]{1,0:T(8,128)(2,1)} %x_in.1, bf16[3,768,512]{2,1,0:T(8,128)(2,1)} %c_in.1, f32[3,128,2048]{2,1,0:T(8,128)} %l_in.1, f32[3,512,128]{2,1,0:T(8,128)} %r_in.1, f32[3,128,512]{2,1,0:T(8,128)} %mom_in.1, ...), custom_call_target="tpu_custom_call" | custom-call | tf_op jit(solution)/shard_map/step/pallas_call | solution.py:392
  182.3 3.2 %put.1 = (f32[3,128,512]{2,1,0:T(8,128)}, f32[3,128,512]{2,1,0:T(8,128)}, bf16[3,4,2,2,2,64,512]{6,5,4,3,2,1,0:T(8,128)(2,1)}) custom-call(f32[3,128,512]{2,1,0:T(8,128)S(1)} %get-tuple-element.9.dir_ref, f32[3,128,512]{2,1,0:T(8,128)S(1)} %get-tuple-element.10.mnew_ref, bf16[3,4,2,2,2,64,512]{6,5,4,3,2,1,0:T(8,128)(2,1)S(1)} %get-tuple-element.11.cf), custom_call_target="tpu_custom_call" | custom-call | tf_op jit(solution)/shard_map/put/pallas_call | solution.py:434
